TPU v7x, 32 devices: a whole 2x2x4 slice. The times are simulated.
32 devices in a mesh: ep: 16 (over z, y, x), tp: 2 (over core).
Axes of the slice: x: 2, y: 2, z: 4, core: 2. Of those that a mesh axis runs over, the one named last changes fastest.
Arguments:
- tokens: bfloat16 [256, 1536], P('ep'), may hold values from -6 to 6
- prior_state: float32 [256, 12, 64, 64], P('ep', 'tp'), may hold values from -12 to 12
- first_gain: float32 [1536], replicated, may hold values from 0.1 to 1.9
- query_weight: bfloat16 [1536, 768], P(None, 'tp'), may hold values from -0.15625 to 0.15625
- key_weight: bfloat16 [1536, 768], P(None, 'tp'), may hold values from -0.15625 to 0.15625
- value_weight: bfloat16 [1536, 768], P(None, 'tp'), may hold values from -0.15625 to 0.15625
- decay_down: bfloat16 [1536, 96], replicated, may hold values from -0.15625 to 0.15625
- decay_up: bfloat16 [96, 768], P(None, 'tp'), may hold values from -1.25 to 1.25
- decay_base: float32 [768], P('tp'), may hold values from -5 to 1
- rate_down: bfloat16 [1536, 96], replicated, may hold values from -0.15625 to 0.15625
- rate_up: bfloat16 [96, 768], P(None, 'tp'), may hold values from -1.25 to 1.25
- rate_base: float32 [768], P('tp'), may hold values from -4 to 4
- head_gain: float32 [768], P('tp'), may hold values from 0.1 to 1.9
- out_weight: bfloat16 [768, 1536], P('tp'), may hold values from -0.21875 to 0.21875
- mid_gain: float32 [1536], replicated, may hold values from 0.1 to 1.9
- route_ids: int32 [256, 6], P('ep'), may hold values from 0 to 15, all different within a row; in each aligned block of 16 rows (0 to 15, 16 to 31, ...) at most 12 rows name the same one
- route_weights: float32 [256, 6], P('ep'), may hold values from 0.1 to 1
- expert_gate: bfloat16 [16, 1536, 384], P('ep', None, 'tp'), may hold values from -0.15625 to 0.15625
- expert_up: bfloat16 [16, 1536, 384], P('ep', None, 'tp'), may hold values from -0.15625 to 0.15625
- expert_down: bfloat16 [16, 384, 1536], P('ep', 'tp'), may hold values from -0.3125 to 0.3125
- dense_gate: bfloat16 [1536, 6144], P(None, ('ep', 'tp')), may hold values from -0.15625 to 0.15625
- dense_up: bfloat16 [1536, 6144], P(None, ('ep', 'tp')), may hold values from -0.15625 to 0.15625
- dense_down: bfloat16 [6144, 1536], P(('ep', 'tp')), may hold values from -0.078125 to 0.078125
- blend_vector: bfloat16 [1536], replicated, may hold values from -0.15625 to 0.15625
Outputs:
- mixed: bfloat16 [256, 1536], P('ep', 'tp')
- new_state: float32 [256, 12, 64, 64], P('ep', 'tp')
Inputs may be any that keep to these rules, and one draw needn't show every extreme that they name: `route_ids`: each row names 6 different experts; among the rows of one device no expert is named by more than 12 rows, a bound that some block reaches.
All inputs are finite; a program needn't handle non-finite values.
Results may differ from a plain program's by a relative error of at most 0.02.
Values may be sent and summed in bfloat16 or wider, within the bound.
No kernel may reach another device: no remote copies, remote signals or barrier semaphores. Data moves between devices by JAX's collectives and lax.ppermute only.
A program may use at most 128 MiB of HBM per device.

v0:
```python
import jax
import jax.numpy as jnp
from jax import lax
from jax.experimental import pallas as pl
from jax.experimental.pallas import tpu as pltpu
from jax.sharding import PartitionSpec as P

BF = jnp.bfloat16
F32 = jnp.float32
MIB = 1024 * 1024
GATHER_TURNS = (3, 1, 2)
REDUCE_TURNS = (3, 2, 1)


VMEM = pl.BlockSpec(memory_space=pltpu.VMEM)
HBM = pl.BlockSpec(memory_space=pltpu.MemorySpace.HBM)


def in_hbm(x):
    return pltpu.with_memory_space_constraint(x, pltpu.MemorySpace.HBM)


def dot(a, b):
    return jnp.dot(a, b, preferred_element_type=F32)


def dot_nt(a, b):
    return lax.dot_general(a, b, (((1,), (1,)), ((), ())), preferred_element_type=F32)


def split(x):
    upper = x.astype(BF)
    return upper, (x - upper.astype(F32)).astype(BF)


def rms_norm(values, gain):
    scale = lax.rsqrt(jnp.mean(values * values, axis=-1, keepdims=True) + 1e-06)
    return values * scale * gain


def mixer_body(heads, head_size, *refs):
    count = 16
    sources, (partial_ref, base_ref, aux_ref, extra_ref) = refs[:count], refs[count : count + 4]
    places, sems = refs[count + 4 : 2 * count + 4], refs[2 * count + 4]
    copies = [pltpu.make_async_copy(sources[at], places[at], sems.at[at]) for at in range(count - 1)]
    state_src, state = sources[count - 1], places[count - 1]
    state_copies = [
        pltpu.make_async_copy(state_src.at[:, h], state.at[h], sems.at[count - 1 + h]) for h in range(heads)
    ]
    (tokens, gain, route_ids, route_weights, key_w, query_w, value_w, decay_down, rate_down, decay_up,
     rate_up, decay_base, rate_base, head_gain, out_w) = places[: count - 1]
    for copy in copies[: count - 2] + state_copies + copies[count - 2 :]:
        copy.start()

    for at in range(2, 4):
        copies[at].wait()
    weights = route_weights[...]
    share = weights / jnp.sum(weights, axis=0, keepdims=True) * 2.5
    upper = share.astype(BF).astype(F32)
    info = jnp.concatenate([route_ids[...].astype(F32), upper, share - upper], axis=0)
    lanes = extra_ref.shape[1]
    info = jnp.concatenate([info, jnp.zeros((lanes - info.shape[0], info.shape[1]), F32)], axis=0)
    extra_ref[...] = info.T.astype(BF)

    seqs = tokens.shape[0]
    copies[0].wait()
    copies[1].wait()
    normed = rms_norm(tokens[...].astype(F32), gain[...]).astype(BF)
    copies[4].wait()
    key = dot(normed, key_w[...]).astype(BF).astype(F32)
    copies[5].wait()
    query = dot(normed, query_w[...]).astype(BF).astype(F32)
    copies[6].wait()
    value = dot(normed, value_w[...]).astype(BF).astype(F32)
    for at in range(7, count - 2):
        copies[at].wait()
    decay_low = jnp.tanh(dot_nt(normed, decay_down[...])).astype(BF)
    decay_log = decay_base[...] + dot(decay_low, decay_up[...])
    decay = jnp.exp(-jnp.exp(-0.5) / (1.0 + jnp.exp(-decay_log)))
    rate_low = dot_nt(normed, rate_down[...]).astype(BF)
    rate = 1.0 / (1.0 + jnp.exp(-(rate_base[...] + dot(rate_low, rate_up[...]))))

    def stacked(x):
        return jnp.concatenate([x[:, h * head_size : (h + 1) * head_size] for h in range(heads)], axis=0)

    def shared(x):
        return jnp.sum(x, axis=-1, keepdims=True)

    key, query, value, decay, rate = (stacked(x) for x in (key, query, value, decay, rate))
    read_upper, read_lower = split(decay * query)
    norm = lax.rsqrt(shared(key * key) + 1e-06)
    unit_rate = key * norm * rate
    removed_part = shared(unit_rate * query)
    value_part = shared(key * query)
    for at, x in ((1, unit_rate), (2, decay), (3, key), (4, value)):
        aux_ref[at] = x.reshape(heads, seqs, head_size)
    key = key.astype(BF)

    cols = seqs * head_size
    row = lax.broadcasted_iota(jnp.int32, (seqs, cols), 0)
    lane = lax.broadcasted_iota(jnp.int32, (seqs, cols), 1)
    own = lane // head_size == row

    def fold(x):
        x = jnp.where(own, x, 0.0)
        while x.shape[1] > 2 * head_size:
            half = x.shape[1] // 2
            x = x[:, :half] + x[:, half:]
        return x

    for copy in state_copies:
        copy.wait()
    removed, kept = [], []
    for h in range(heads):
        cut = slice(h * seqs, (h + 1) * seqs)
        rows = jnp.concatenate([key[cut], read_upper[cut], read_lower[cut]], axis=0)
        upper, lower = split(state[h].reshape(cols, head_size))
        both = dot_nt(rows, upper) + dot_nt(rows, lower)
        removed.append(fold(both[:seqs]))
        kept.append(fold(both[seqs : 2 * seqs] + both[2 * seqs :]))
    removed, kept = (jnp.concatenate(x, axis=0) for x in (removed, kept))
    removed = (removed[:, :head_size] + removed[:, head_size:]) * norm
    kept = kept[:, :head_size] + kept[:, head_size:]
    aux_ref[0] = removed.reshape(heads, seqs, head_size)
    read = kept - removed * removed_part + value * value_part
    read = read - jnp.mean(read, axis=-1, keepdims=True)
    read = read * lax.rsqrt(jnp.mean(read * read, axis=-1, keepdims=True) + 0.00064)
    pieces = [read[h * seqs : (h + 1) * seqs] for h in range(heads)]
    mixed = (jnp.concatenate(pieces, axis=1) * head_gain[...]).astype(BF)
    copies[count - 2].wait()
    partial = dot(mixed, out_w[...]).astype(BF)
    partial_ref[...] = partial
    base_ref[...] = tokens[...].astype(F32) + partial.astype(F32)


def mixer(*args):
    seqs, heads, _, head_size = args[-1].shape
    width = args[0].shape[1]
    scratch = [pltpu.VMEM(a.shape, a.dtype) for a in args[:-1]]
    scratch.append(pltpu.VMEM((heads, seqs, head_size, head_size), F32))
    scratch.append(pltpu.SemaphoreType.DMA((len(args) + heads,)))
    return pl.pallas_call(
        lambda *refs: mixer_body(heads, head_size, *refs),
        out_shape=(
            pltpu.VMEM((seqs, width), BF),
            pltpu.VMEM((seqs, width), F32),
            pltpu.VMEM((5, heads, seqs, head_size), F32),
            pltpu.VMEM((seqs, 128), BF),
        ),
        in_specs=[HBM] * len(args),
        out_specs=(VMEM,) * 4,
        scratch_shapes=scratch,
        compiler_params=pltpu.CompilerParams(vmem_limit_bytes=16 * MIB),
        name="mixer",
    )(*(in_hbm(a) for a in args))


def state_body(state_ref, aux_ref, new_ref):
    seqs, _, size, _ = state_ref.shape
    cols = seqs * size
    removed, unit_rate, decay, key, value = (aux_ref[i, pl.program_id(0)] for i in range(5))
    removed_upper, removed_lower = (x.astype(F32) for x in split(removed))
    rate_upper, rate_lower = split(-unit_rate)
    left = jnp.concatenate([removed_upper, removed_lower, removed_upper, value], axis=0)
    right = jnp.concatenate([rate_upper, rate_upper, rate_lower, key.astype(BF)], axis=0)
    row = lax.broadcasted_iota(jnp.int32, (4 * seqs, cols), 0)
    lane = lax.broadcasted_iota(jnp.int32, (4 * seqs, cols), 1)
    left = jnp.where(lane // size == row % seqs, jnp.concatenate([left] * seqs, axis=1), 0.0)
    outer = dot(left.T.astype(BF), right)
    new_ref[:, 0] = state_ref[:, 0] * decay[:, None, :] + outer.reshape(seqs, size, size)


def update_state(state, aux):
    seqs, heads, size, _ = state.shape
    block = pl.BlockSpec((seqs, 1, size, size), lambda h: (0, h, 0, 0))
    return pl.pallas_call(
        state_body,
        grid=(heads,),
        out_shape=jax.ShapeDtypeStruct(state.shape, F32),
        in_specs=[block, VMEM],
        out_specs=block,
        cost_estimate=pl.CostEstimate(
            flops=4 * 64 * state.size, transcendentals=0, bytes_accessed=16 * state.size
        ),
        compiler_params=pltpu.CompilerParams(vmem_limit_bytes=16 * MIB),
        name="state_update",
    )(state, aux)


def pack_body(top, half, base, other, gain, blend_vector, extra, block_ref, resid_ref):
    resid = (base[...] + other[...].astype(F32)).astype(BF).astype(F32)
    mid = rms_norm(resid, gain[...]).astype(BF)
    score = jnp.sum(mid.astype(F32) * blend_vector[...].astype(F32), axis=-1, keepdims=True)
    upper, lower = (x.astype(F32) for x in split(1.0 / (1.0 + jnp.exp(-score))))
    info = extra[...].astype(F32)
    lane = lax.broadcasted_iota(jnp.int32, info.shape, 1)
    info = jnp.where(lane == 3 * top, upper, jnp.where(lane == 3 * top + 1, lower, info))
    first = lax.axis_index("tp") == 0
    block_ref[:, :half] = jnp.where(first, mid[:, :half], mid[:, half:])
    block_ref[:, half:] = info.astype(BF)
    resid_ref[...] = jnp.where(first, resid[:, :half], resid[:, half:])


def pack(base, other, gain, blend_vector, extra, top):
    seqs, width = base.shape
    half = width // 2
    return pl.pallas_call(
        lambda *refs: pack_body(top, half, *refs),
        out_shape=(
            pltpu.VMEM((seqs, half + extra.shape[1]), BF),
            pltpu.VMEM((seqs, half), F32),
        ),
        in_specs=[VMEM] * 5,
        out_specs=(VMEM, VMEM),
        compiler_params=pltpu.CompilerParams(vmem_limit_bytes=4 * MIB),
        name="pack",
    )(base, other, gain, blend_vector, extra)


def ffn_body(pieces, seqs, top, half, *refs):
    places, blocks = refs[:6], refs[6 : 6 + 2 * pieces]
    other_ref, mine_ref = refs[6 + 2 * pieces :]
    near = jnp.concatenate([b[:, :half] for b in blocks[:pieces]], axis=0)
    far = jnp.concatenate([b[:, :half] for b in blocks[pieces:]], axis=0)
    first = lax.axis_index("tp") == 0
    rows = jnp.concatenate([jnp.where(first, near, far), jnp.where(first, far, near)], axis=1)
    info = jnp.concatenate([b[:, half:] for b in blocks[:pieces]], axis=0).astype(F32)
    scalars = info[:, top : 2 * top] + info[:, 2 * top : 3 * top]
    here = lax.axis_index("ep").astype(F32)
    scale = jnp.sum(jnp.where(info[:, :top] == here, scalars, 0.0), axis=1, keepdims=True)
    blend = info[:, 3 * top : 3 * top + 1] + info[:, 3 * top + 1 : 3 * top + 2]

    def hidden(at, by):
        gate = dot_nt(rows, places[at][...])
        up = dot_nt(rows, places[at + 1][...])
        return (gate / (1.0 + jnp.exp(-gate)) * up * by).astype(BF)

    expert = hidden(0, scale)
    dense = hidden(2, blend)
    count = blocks[0].shape[0] // seqs
    chunk = lax.broadcasted_iota(jnp.int32, (near.shape[0], 1), 0) // seqs % count
    side = chunk * 0 + lax.axis_index("tp")
    for bit in range(count.bit_length() - 1):
        side = side ^ (chunk >> bit & 1)
    low = dot(expert, places[4][:, :half]) + dot(dense, places[5][:, :half])
    high = dot(expert, places[4][:, half:]) + dot(dense, places[5][:, half:])
    other_ref[...] = jnp.where(side == 0, high, low).astype(BF)
    mine_ref[...] = jnp.where(side == 0, low, high)


def ffn(weights, near, far, seqs, top):
    rows = sum(b.shape[0] for b in near)
    half = weights[-1].shape[1] // 2
    return pl.pallas_call(
        lambda *refs: ffn_body(len(near), seqs, top, half, *refs),
        out_shape=(pltpu.VMEM((rows, half), BF), pltpu.VMEM((rows, half), F32)),
        in_specs=[VMEM] * (len(weights) + 2 * len(near)),
        out_specs=(VMEM, VMEM),
        compiler_params=pltpu.CompilerParams(vmem_limit_bytes=8 * MIB + rows * 20 * 1024),
        name="ffn",
    )(*weights, *near, *far)


def swap_tp(x):
    count = lax.axis_size("tp")
    return lax.ppermute(x, "tp", [(i, i ^ 1) for i in range(count)])


def cross(x, mask):
    size = lax.axis_size("tp")
    pairs = [
        (i * size + j, (i ^ mask) * size + (j ^ 1)) for i in range(lax.axis_size("ep")) for j in range(size)
    ]
    return lax.ppermute(x, ("ep", "tp"), pairs)


def swap_ep(x, mask):
    count = lax.axis_size("ep")
    return lax.ppermute(x, "ep", [(i, i ^ mask) for i in range(count)])


def shards(
    tokens,
    prior_state,
    first_gain,
    query_weight,
    key_weight,
    value_weight,
    decay_down,
    decay_up,
    decay_base,
    rate_down,
    rate_up,
    rate_base,
    head_gain,
    out_weight,
    mid_gain,
    route_ids,
    route_weights,
    expert_gate,
    expert_up,
    expert_down,
    dense_gate,
    dense_up,
    dense_down,
    blend_vector,
):
    count_ep = lax.axis_size("ep")
    seqs = tokens.shape[0]
    width = tokens.shape[1]
    top_count = route_ids.shape[1]
    half_width = width // 2
    partial_value, base, aux, extra = mixer(
        tokens,
        first_gain,
        route_ids.T,
        route_weights.T,
        key_weight,
        query_weight,
        value_weight,
        decay_down.T,
        rate_down.T,
        decay_up,
        rate_up,
        decay_base,
        rate_base,
        head_gain,
        out_weight,
        prior_state,
    )
    block, resid = pack(base, swap_tp(partial_value), mid_gain, blend_vector, extra, top_count)

    mask = count_ep // 2
    masks = []
    while mask >= 4:
        block = jnp.concatenate([block, swap_ep(block, mask)], axis=0)
        masks.append(mask)
        mask //= 2
    low = [m for m in (1, 3, 2) if m < count_ep]
    near = [block]
    for m in low:
        near.append(swap_ep(block, m))
    far = [swap_tp(b) for b in near]
    rows = sum(b.shape[0] for b in near)

    weights = (
        expert_gate[0].T,
        expert_up[0].T,
        dense_gate.T,
        dense_up.T,
        expert_down[0],
        dense_down,
    )
    other, mine = ffn(weights, near, far, seqs, top_count)
    total = mine + swap_tp(other).astype(F32)

    groups = len(low) + 1
    part = total.reshape((groups, rows // groups, half_width))
    send, aux = lax.optimization_barrier((part.astype(BF), aux))
    new_state = update_state(prior_state, aux)
    back = []
    for i, m in enumerate(low):
        back.append(swap_ep(send[i + 1], m))
    back, new_state = lax.optimization_barrier((back, new_state))
    total = part[0] + sum(x.astype(F32) for x in back)
    for mask in reversed(masks):
        part = total.reshape((2, -1, half_width))
        total = part[0] + cross(part[1].astype(BF), mask).astype(F32)

    mixed = (resid + total).astype(BF)
    return (mixed, new_state)


def solution(mesh):
    in_specs = (
        P("ep", None),
        P("ep", "tp", None, None),
        P(),
        P(None, "tp"),
        P(None, "tp"),
        P(None, "tp"),
        P(),
        P(None, "tp"),
        P("tp"),
        P(),
        P(None, "tp"),
        P("tp"),
        P("tp"),
        P("tp", None),
        P(),
        P("ep", None),
        P("ep", None),
        P("ep", None, "tp"),
        P("ep", None, "tp"),
        P("ep", "tp", None),
        P(None, ("ep", "tp")),
        P(None, ("ep", "tp")),
        P(("ep", "tp"), None),
        P(),
    )
    out_specs = (P("ep", "tp"), P("ep", "tp", None, None))
    step = jax.shard_map(shards, mesh=mesh, in_specs=in_specs, out_specs=out_specs, check_vma=False)
    for turns in (GATHER_TURNS, REDUCE_TURNS):
        turns = [m for m in turns if m < mesh.shape["ep"]]
    return step
```

profile of v0, /device:TPU:0, one launch (start us, length us, event | category | flops | bytes accessed | tf_op | source)
XLA Modules:
  0.0 48.4 jit_solution(3109309359197312453)
XLA Ops:
  0.7 5.4 %mixer.1 = (bf16[16,1536]{1,0:T(8,128)(2,1)S(1)}, f32[16,1536]{1,0:T(8,128)S(1)}, f32[5,6,16,64]{3,2,1,0:T(8,128)S(1)}, bf16[16,128]{1,0:T(8,128)(2,1)S(1)}) custom-call(bf16[16,1536]{1,0:T(8,128)(2,1)} %refs_0_.1, f32[1536]{0:T(1024)} %refs_1_.1, s32[6,16]{1,0:T(8,128)} %bitcast.28, f32[6,16]{1,0:T(8,128)} %bitcast.29, bf16[1536,384]{1,0:T(8,128)(2,1)} %refs_4_.1, ...), custom_call_target="tpu_custom_call" | custom-call | tf_op jit(solution)/shard_map/mixer/pallas_call | solution.py:142
  6.1 0.6 %collective-permute-start = (bf16[16,1536]{1,0:T(8,128)(2,1)S(1)}, bf16[16,1536]{1,0:T(8,128)(2,1)S(1)}, u32[]{:S(2)}, u32[]{:S(2)}) collective-permute-start(bf16[16,1536]{1,0:T(8,128)(2,1)S(1)} %get-tuple-element.17), channel_id=1, source_target_pairs={{0,1},{1,0},{2,3},{3,2},{4,5},{5,4},{6,7},{7,6},{8,9},{9,8},{10,11... | collective-permute-start | bytes 147464 | tf_op jit(solution)/shard_map/ppermute | solution.py:266
  6.7 0.9 %collective-permute-done.refs_1_ = bf16[16,1536]{1,0:T(8,128)(2,1)S(1)} collective-permute-done((bf16[16,1536]{1,0:T(8,128)(2,1)S(1)}, bf16[16,1536]{1,0:T(8,128)(2,1)S(1)}, u32[]{:S(2)}, u32[]{:S(2)}) %collective-permute-start) | collective-permute-done | bytes 49184 | tf_op jit(solution)/shard_map/ppermute | solution.py:266
  7.6 0.2 pack.1
  7.8 4.0 %collective-permute-start.1 = (bf16[16,896]{1,0:T(8,128)(2,1)S(1)}, bf16[16,896]{1,0:T(8,128)(2,1)S(1)}, u32[]{:S(2)}, u32[]{:S(2)}) collective-permute-start(bf16[16,896]{1,0:T(8,128)(2,1)S(1)} %get-tuple-element.20), channel_id=1, source_target_pairs={{0,16},{2,18},{4,20},{6,22},{8,24},{10,26},{12,28},{14,30},{16,0},... | collective-permute-start | bytes 86024 | tf_op jit(solution)/shard_map/ppermute | solution.py:279
  11.8 1.8 %collective-permute-done.1 = bf16[16,896]{1,0:T(8,128)(2,1)S(1)} collective-permute-done((bf16[16,896]{1,0:T(8,128)(2,1)S(1)}, bf16[16,896]{1,0:T(8,128)(2,1)S(1)}, u32[]{:S(2)}, u32[]{:S(2)}) %collective-permute-start.1) | collective-permute-done | bytes 28704 | tf_op jit(solution)/shard_map/ppermute | solution.py:279
  13.6 1.9 %collective-permute-start.2 = (bf16[32,896]{1,0:T(8,128)(2,1)S(1)}, bf16[32,896]{1,0:T(8,128)(2,1)S(1)}, u32[]{:S(2)}, u32[]{:S(2)}) collective-permute-start(bf16[32,896]{1,0:T(8,128)(2,1)S(1)} %pad_maximum_fusion), channel_id=1, source_target_pairs={{0,8},{2,10},{4,12},{6,14},{8,0},{10,2},{12,4},{14,6},{16,24},{18,... | collective-permute-start | bytes 172040 | tf_op jit(solution)/shard_map/ppermute | solution.py:279
  15.6 2.3 %collective-permute-done.2 = bf16[32,896]{1,0:T(8,128)(2,1)S(1)} collective-permute-done((bf16[32,896]{1,0:T(8,128)(2,1)S(1)}, bf16[32,896]{1,0:T(8,128)(2,1)S(1)}, u32[]{:S(2)}, u32[]{:S(2)}) %collective-permute-start.2) | collective-permute-done | bytes 57376 | tf_op jit(solution)/shard_map/ppermute | solution.py:279
  17.8 1.9 %collective-permute-start.5 = (bf16[64,896]{1,0:T(8,128)(2,1)S(1)}, bf16[64,896]{1,0:T(8,128)(2,1)S(1)}, u32[]{:S(2)}, u32[]{:S(2)}) collective-permute-start(bf16[64,896]{1,0:T(8,128)(2,1)S(1)} %constant_dynamic-update-slice_fusion.refs_6_), channel_id=1, source_target_pairs={{0,4},{2,6},{4,0},{6,2},{8,12},{10,14},{12,8},{14,10},{16,20},{18,... | collective-permute-start | bytes 344072 | tf_op jit(solution)/shard_map/ppermute | solution.py:279
  19.8 1.7 %collective-permute-start.4 = (bf16[64,896]{1,0:T(8,128)(2,1)S(1)}, bf16[64,896]{1,0:T(8,128)(2,1)S(1)}, u32[]{:S(2)}, u32[]{:S(2)}) collective-permute-start(bf16[64,896]{1,0:T(8,128)(2,1)S(1)} %constant_dynamic-update-slice_fusion.refs_6_), channel_id=1, source_target_pairs={{0,6},{2,4},{4,2},{6,0},{8,14},{10,12},{12,10},{14,8},{16,22},{18,... | collective-permute-start | bytes 344072 | tf_op jit(solution)/shard_map/ppermute | solution.py:279
  21.5 0.1 collective-permute-start.3
  21.6 1.7 %collective-permute-done.5.refs_9_ = bf16[64,896]{1,0:T(8,128)(2,1)S(1)} collective-permute-done((bf16[64,896]{1,0:T(8,128)(2,1)S(1)}, bf16[64,896]{1,0:T(8,128)(2,1)S(1)}, u32[]{:S(2)}, u32[]{:S(2)}) %collective-permute-start.5) | collective-permute-done | bytes 114720 | tf_op jit(solution)/shard_map/ppermute | solution.py:279
  23.3 2.2 %collective-permute-done.4.refs_8_ = bf16[64,896]{1,0:T(8,128)(2,1)S(1)} collective-permute-done((bf16[64,896]{1,0:T(8,128)(2,1)S(1)}, bf16[64,896]{1,0:T(8,128)(2,1)S(1)}, u32[]{:S(2)}, u32[]{:S(2)}) %collective-permute-start.4) | collective-permute-done | bytes 114720 | tf_op jit(solution)/shard_map/ppermute | solution.py:279
  25.4 0.8 %collective-permute-done.3.refs_7_ = bf16[64,896]{1,0:T(8,128)(2,1)S(1)} collective-permute-done((bf16[64,896]{1,0:T(8,128)(2,1)S(1)}, bf16[64,896]{1,0:T(8,128)(2,1)S(1)}, u32[]{:S(2)}, u32[]{:S(2)}) %collective-permute-start.3) | collective-permute-done | bytes 114720 | tf_op jit(solution)/shard_map/ppermute | solution.py:279
  26.3 0.5 collective-permute-done.8.refs_12_
  26.8 0.8 %collective-permute-done.7.refs_11_ = bf16[64,896]{1,0:T(8,128)(2,1)S(1)} collective-permute-done((bf16[64,896]{1,0:T(8,128)(2,1)S(1)}, bf16[64,896]{1,0:T(8,128)(2,1)S(1)}, u32[]{:S(2)}, u32[]{:S(2)}) %collective-permute-start.7) | collective-permute-done | bytes 114720 | tf_op jit(solution)/shard_map/ppermute | solution.py:266
  27.6 0.0 copy-start
  27.7 1.5 %ffn.1 = (bf16[256,768]{1,0:T(8,128)(2,1)S(1)}, f32[256,768]{1,0:T(8,128)S(1)}) custom-call(bf16[192,1536]{1,0:T(8,128)(2,1)S(1)} %bitcast.20, bf16[192,1536]{1,0:T(8,128)(2,1)S(1)} %bitcast.21, bf16[192,1536]{1,0:T(8,128)(2,1)S(1)} %bitcast.22, bf16[192,1536]{1,0:T(8,128)(2,1)S(1)} %bitcast.23, bf16[192,1536]{1,0:T(8,128)(2,1)S(1)} %bitcast.24, ...), custom_call_target="tpu_custom_call" | custom-call | tf_op jit(solution)/shard_map/ffn/pallas_call | solution.py:254
  29.2 0.2 collective-permute-start.10
  29.4 1.6 %collective-permute-done.10 = bf16[256,768]{1,0:T(8,128)(2,1)S(1)} collective-permute-done((bf16[256,768]{1,0:T(8,128)(2,1)S(1)}, bf16[256,768]{1,0:T(8,128)(2,1)S(1)}, u32[]{:S(2)}, u32[]{:S(2)}) %collective-permute-start.10) | collective-permute-done | bytes 393248 | tf_op jit(solution)/shard_map/ppermute | solution.py:266
  31.0 0.1 fusion.2
  31.1 1.6 %collective-permute-start.13 = (bf16[64,768]{1,0:T(8,128)(2,1)S(1)}, bf16[64,768]{1,0:T(8,128)(2,1)S(1)}, u32[]{:S(2)}, u32[]{:S(2)}) collective-permute-start(bf16[64,768]{1,0:T(8,128)(2,1)S(1)} %get-tuple-element.32), channel_id=1, source_target_pairs={{0,4},{2,6},{4,0},{6,2},{8,12},{10,14},{12,8},{14,10},{16,20},{18,... | collective-permute-start | bytes 294920 | tf_op jit(solution)/shard_map/ppermute | solution.py:279
  32.7 1.2 %collective-permute-start.12 = (bf16[64,768]{1,0:T(8,128)(2,1)S(1)}, bf16[64,768]{1,0:T(8,128)(2,1)S(1)}, u32[]{:S(2)}, u32[]{:S(2)}) collective-permute-start(bf16[64,768]{1,0:T(8,128)(2,1)S(1)} %get-tuple-element.33), channel_id=1, source_target_pairs={{0,6},{2,4},{4,2},{6,0},{8,14},{10,12},{12,10},{14,8},{16,22},{18,... | collective-permute-start | bytes 294920 | tf_op jit(solution)/shard_map/ppermute | solution.py:279
  33.9 0.8 %collective-permute-start.11 = (bf16[64,768]{1,0:T(8,128)(2,1)S(1)}, bf16[64,768]{1,0:T(8,128)(2,1)S(1)}, u32[]{:S(2)}, u32[]{:S(2)}) collective-permute-start(bf16[64,768]{1,0:T(8,128)(2,1)S(1)} %get-tuple-element.34), channel_id=1, source_target_pairs={{0,2},{2,0},{4,6},{6,4},{8,10},{10,8},{12,14},{14,12},{16,18},{18,... | collective-permute-start | bytes 294920 | tf_op jit(solution)/shard_map/ppermute | solution.py:279
  34.7 4.1 %state_update.1 = f32[16,6,64,64]{3,2,1,0:T(8,128)} custom-call(f32[16,6,64,64]{3,2,1,0:T(8,128)S(1)} %copy-done, f32[5,6,16,64]{3,2,1,0:T(8,128)S(1)} %get-tuple-element.25.aux_ref), custom_call_target="tpu_custom_call" | custom-call | flops 100663296 | bytes 6291456 | tf_op jit(solution)/shard_map/state_update/pallas_call | solution.py:176
  38.7 0.5 %collective-permute-done.12 = bf16[64,768]{1,0:T(8,128)(2,1)S(1)} collective-permute-done((bf16[64,768]{1,0:T(8,128)(2,1)S(1)}, bf16[64,768]{1,0:T(8,128)(2,1)S(1)}, u32[]{:S(2)}, u32[]{:S(2)}) %collective-permute-start.12) | collective-permute-done | bytes 98336 | tf_op jit(solution)/shard_map/ppermute | solution.py:279
  39.2 0.1 collective-permute-done.11
  39.4 0.1 collective-permute-start.14
  39.5 3.8 %collective-permute-done.14 = bf16[32,768]{1,0:T(8,128)(2,1)S(1)} collective-permute-done((bf16[32,768]{1,0:T(8,128)(2,1)S(1)}, bf16[32,768]{1,0:T(8,128)(2,1)S(1)}, u32[]{:S(2)}, u32[]{:S(2)}) %collective-permute-start.14) | collective-permute-done | bytes 49184 | tf_op jit(solution)/shard_map/ppermute | solution.py:274
  43.4 2.0 %collective-permute-start.15 = (bf16[16,768]{1,0:T(8,128)(2,1)S(1)}, bf16[16,768]{1,0:T(8,128)(2,1)S(1)}, u32[]{:S(2)}, u32[]{:S(2)}) collective-permute-start(bf16[16,768]{1,0:T(8,128)(2,1)S(1)} %slice.57), channel_id=1, source_target_pairs={{0,17},{1,16},{2,19},{3,18},{4,21},{5,20},{6,23},{7,22},{8,25},{9,... | collective-permute-start | bytes 73736 | tf_op jit(solution)/shard_map/ppermute | solution.py:274
  45.3 2.4 %collective-permute-done.15 = bf16[16,768]{1,0:T(8,128)(2,1)S(1)} collective-permute-done((bf16[16,768]{1,0:T(8,128)(2,1)S(1)}, bf16[16,768]{1,0:T(8,128)(2,1)S(1)}, u32[]{:S(2)}, u32[]{:S(2)}) %collective-permute-start.15) | collective-permute-done | bytes 24608 | tf_op jit(solution)/shard_map/ppermute | solution.py:274
  47.8 0.6 %fusion.1 = bf16[16,768]{1,0:T(8,128)(2,1)} fusion(f32[16,768]{1,0:T(8,128)S(1)} %get-tuple-element.19, f32[32,768]{1,0:T(8,128)S(1)} %slice_add_fusion.1, bf16[16,768]{1,0:T(8,128)(2,1)S(1)} %collective-permute-done.15), kind=kLoop, calls=%fused_computation.11 | loop fusion | flops 49152 | bytes 147456 | tf_op jit(solution)/shard_map/convert_element_type | solution.py:370
  (33 shorter events, 0.2 us)
Async XLA Ops:
  0.6 6.9 %copy-start.7 = (f32[1536]{0:T(1024)S(1)}, f32[1536]{0:T(1024)}, u32[]{:S(2)}) copy-start(f32[1536]{0:T(1024)} %refs_2_.1) | copy-start | bytes 18436
  0.6 6.9 %copy-start.8 = (bf16[1536]{0:T(1024)(128)(2,1)S(1)}, bf16[1536]{0:T(1024)(128)(2,1)}, u32[]{:S(2)}) copy-start(bf16[1536]{0:T(1024)(128)(2,1)} %refs_3_.1) | copy-start | bytes 9220
  0.7 26.9 %copy-start.1 = (bf16[1,1536,192]{1,2,0:T(8,128)(2,1)S(1)}, bf16[1,1536,192]{1,2,0:T(8,128)(2,1)}, u32[]{:S(2)}) copy-start(bf16[1,1536,192]{1,2,0:T(8,128)(2,1)} %param.41) | copy-start | bytes 1769476
  0.7 26.9 %copy-start.2 = (bf16[1,1536,192]{1,2,0:T(8,128)(2,1)S(1)}, bf16[1,1536,192]{1,2,0:T(8,128)(2,1)}, u32[]{:S(2)}) copy-start(bf16[1,1536,192]{1,2,0:T(8,128)(2,1)} %param.42) | copy-start | bytes 1769476
  0.7 26.9 %copy-start.3 = (bf16[1536,192]{0,1:T(8,128)(2,1)S(1)}, bf16[1536,192]{0,1:T(8,128)(2,1)}, u32[]{:S(2)}) copy-start(bf16[1536,192]{0,1:T(8,128)(2,1)} %param.44) | copy-start | bytes 1769476
  0.7 26.9 %copy-start.4 = (bf16[1536,192]{0,1:T(8,128)(2,1)S(1)}, bf16[1536,192]{0,1:T(8,128)(2,1)}, u32[]{:S(2)}) copy-start(bf16[1536,192]{0,1:T(8,128)(2,1)} %param.45) | copy-start | bytes 1769476
  0.7 26.9 %copy-start.5 = (bf16[1,192,1536]{2,1,0:T(8,128)(2,1)S(1)}, bf16[1,192,1536]{2,1,0:T(8,128)(2,1)}, u32[]{:S(2)}) copy-start(bf16[1,192,1536]{2,1,0:T(8,128)(2,1)} %param.43) | copy-start | bytes 1769476
  0.7 26.9 %copy-start.6 = (bf16[192,1536]{1,0:T(8,128)(2,1)S(1)}, bf16[192,1536]{1,0:T(8,128)(2,1)}, u32[]{:S(2)}) copy-start(bf16[192,1536]{1,0:T(8,128)(2,1)} %refs_5_.3) | copy-start | bytes 1769476
  6.1 1.4 %collective-permute-start = (bf16[16,1536]{1,0:T(8,128)(2,1)S(1)}, bf16[16,1536]{1,0:T(8,128)(2,1)S(1)}, u32[]{:S(2)}, u32[]{:S(2)}) collective-permute-start(bf16[16,1536]{1,0:T(8,128)(2,1)S(1)} %get-tuple-element.17), channel_id=1, source_target_pairs={{0,1},{1,0},{2,3},{3,2},{4,5},{5,4},{6,7},{7,6},{8,9},{9,8},{10,11... | collective-permute-start | bytes 147464 | tf_op jit(solution)/shard_map/ppermute | solution.py:266
  7.8 5.8 %collective-permute-start.1 = (bf16[16,896]{1,0:T(8,128)(2,1)S(1)}, bf16[16,896]{1,0:T(8,128)(2,1)S(1)}, u32[]{:S(2)}, u32[]{:S(2)}) collective-permute-start(bf16[16,896]{1,0:T(8,128)(2,1)S(1)} %get-tuple-element.20), channel_id=1, source_target_pairs={{0,16},{2,18},{4,20},{6,22},{8,24},{10,26},{12,28},{14,30},{16,0},... | collective-permute-start | bytes 86024 | tf_op jit(solution)/shard_map/ppermute | solution.py:279
  13.6 4.2 %collective-permute-start.2 = (bf16[32,896]{1,0:T(8,128)(2,1)S(1)}, bf16[32,896]{1,0:T(8,128)(2,1)S(1)}, u32[]{:S(2)}, u32[]{:S(2)}) collective-permute-start(bf16[32,896]{1,0:T(8,128)(2,1)S(1)} %pad_maximum_fusion), channel_id=1, source_target_pairs={{0,8},{2,10},{4,12},{6,14},{8,0},{10,2},{12,4},{14,6},{16,24},{18,... | collective-permute-start | bytes 172040 | tf_op jit(solution)/shard_map/ppermute | solution.py:279
  17.8 5.4 %collective-permute-start.5 = (bf16[64,896]{1,0:T(8,128)(2,1)S(1)}, bf16[64,896]{1,0:T(8,128)(2,1)S(1)}, u32[]{:S(2)}, u32[]{:S(2)}) collective-permute-start(bf16[64,896]{1,0:T(8,128)(2,1)S(1)} %constant_dynamic-update-slice_fusion.refs_6_), channel_id=1, source_target_pairs={{0,4},{2,6},{4,0},{6,2},{8,12},{10,14},{12,8},{14,10},{16,20},{18,... | collective-permute-start | bytes 344072 | tf_op jit(solution)/shard_map/ppermute | solution.py:279
  19.8 5.7 %collective-permute-start.4 = (bf16[64,896]{1,0:T(8,128)(2,1)S(1)}, bf16[64,896]{1,0:T(8,128)(2,1)S(1)}, u32[]{:S(2)}, u32[]{:S(2)}) collective-permute-start(bf16[64,896]{1,0:T(8,128)(2,1)S(1)} %constant_dynamic-update-slice_fusion.refs_6_), channel_id=1, source_target_pairs={{0,6},{2,4},{4,2},{6,0},{8,14},{10,12},{12,10},{14,8},{16,22},{18,... | collective-permute-start | bytes 344072 | tf_op jit(solution)/shard_map/ppermute | solution.py:279
  21.5 4.8 %collective-permute-start.3 = (bf16[64,896]{1,0:T(8,128)(2,1)S(1)}, bf16[64,896]{1,0:T(8,128)(2,1)S(1)}, u32[]{:S(2)}, u32[]{:S(2)}) collective-permute-start(bf16[64,896]{1,0:T(8,128)(2,1)S(1)} %constant_dynamic-update-slice_fusion.refs_6_), channel_id=1, source_target_pairs={{0,2},{2,0},{4,6},{6,4},{8,10},{10,8},{12,14},{14,12},{16,18},{18,... | collective-permute-start | bytes 344072 | tf_op jit(solution)/shard_map/ppermute | solution.py:279
  21.6 4.7 %collective-permute-start.6 = (bf16[64,896]{1,0:T(8,128)(2,1)S(1)}, bf16[64,896]{1,0:T(8,128)(2,1)S(1)}, u32[]{:S(2)}, u32[]{:S(2)}) collective-permute-start(bf16[64,896]{1,0:T(8,128)(2,1)S(1)} %constant_dynamic-update-slice_fusion.refs_6_), channel_id=1, source_target_pairs={{0,1},{1,0},{2,3},{3,2},{4,5},{5,4},{6,7},{7,6},{8,9},{9,8},{10,11... | collective-permute-start | bytes 344072 | tf_op jit(solution)/shard_map/ppermute | solution.py:266
  23.3 3.0 %collective-permute-start.9 = (bf16[64,896]{1,0:T(8,128)(2,1)S(1)}, bf16[64,896]{1,0:T(8,128)(2,1)S(1)}, u32[]{:S(2)}, u32[]{:S(2)}) collective-permute-start(bf16[64,896]{1,0:T(8,128)(2,1)S(1)} %collective-permute-done.5.refs_9_), channel_id=1, source_target_pairs={{0,1},{1,0},{2,3},{3,2},{4,5},{5,4},{6,7},{7,6},{8,9},{9,8},{10,11... | collective-permute-start | bytes 344072 | tf_op jit(solution)/shard_map/ppermute | solution.py:266
  25.4 1.3 %collective-permute-start.8 = (bf16[64,896]{1,0:T(8,128)(2,1)S(1)}, bf16[64,896]{1,0:T(8,128)(2,1)S(1)}, u32[]{:S(2)}, u32[]{:S(2)}) collective-permute-start(bf16[64,896]{1,0:T(8,128)(2,1)S(1)} %collective-permute-done.4.refs_8_), channel_id=1, source_target_pairs={{0,1},{1,0},{2,3},{3,2},{4,5},{5,4},{6,7},{7,6},{8,9},{9,8},{10,11... | collective-permute-start | bytes 344072 | tf_op jit(solution)/shard_map/ppermute | solution.py:266
  26.3 1.3 %collective-permute-start.7 = (bf16[64,896]{1,0:T(8,128)(2,1)S(1)}, bf16[64,896]{1,0:T(8,128)(2,1)S(1)}, u32[]{:S(2)}, u32[]{:S(2)}) collective-permute-start(bf16[64,896]{1,0:T(8,128)(2,1)S(1)} %collective-permute-done.3.refs_7_), channel_id=1, source_target_pairs={{0,1},{1,0},{2,3},{3,2},{4,5},{5,4},{6,7},{7,6},{8,9},{9,8},{10,11... | collective-permute-start | bytes 344072 | tf_op jit(solution)/shard_map/ppermute | solution.py:266
  27.6 7.0 %copy-start = (f32[16,6,64,64]{3,2,1,0:T(8,128)S(1)}, f32[16,6,64,64]{3,2,1,0:T(8,128)}, u32[]{:S(2)}) copy-start(f32[16,6,64,64]{3,2,1,0:T(8,128)} %state_ref.1) | copy-start | bytes 4718596
  29.2 1.8 %collective-permute-start.10 = (bf16[256,768]{1,0:T(8,128)(2,1)S(1)}, bf16[256,768]{1,0:T(8,128)(2,1)S(1)}, u32[]{:S(2)}, u32[]{:S(2)}) collective-permute-start(bf16[256,768]{1,0:T(8,128)(2,1)S(1)} %get-tuple-element.22), channel_id=1, source_target_pairs={{0,1},{1,0},{2,3},{3,2},{4,5},{5,4},{6,7},{7,6},{8,9},{9,8},{10,11... | collective-permute-start | bytes 1179656 | tf_op jit(solution)/shard_map/ppermute | solution.py:266
  31.1 7.6 %collective-permute-start.13 = (bf16[64,768]{1,0:T(8,128)(2,1)S(1)}, bf16[64,768]{1,0:T(8,128)(2,1)S(1)}, u32[]{:S(2)}, u32[]{:S(2)}) collective-permute-start(bf16[64,768]{1,0:T(8,128)(2,1)S(1)} %get-tuple-element.32), channel_id=1, source_target_pairs={{0,4},{2,6},{4,0},{6,2},{8,12},{10,14},{12,8},{14,10},{16,20},{18,... | collective-permute-start | bytes 294920 | tf_op jit(solution)/shard_map/ppermute | solution.py:279
  32.7 6.5 %collective-permute-start.12 = (bf16[64,768]{1,0:T(8,128)(2,1)S(1)}, bf16[64,768]{1,0:T(8,128)(2,1)S(1)}, u32[]{:S(2)}, u32[]{:S(2)}) collective-permute-start(bf16[64,768]{1,0:T(8,128)(2,1)S(1)} %get-tuple-element.33), channel_id=1, source_target_pairs={{0,6},{2,4},{4,2},{6,0},{8,14},{10,12},{12,10},{14,8},{16,22},{18,... | collective-permute-start | bytes 294920 | tf_op jit(solution)/shard_map/ppermute | solution.py:279
  33.9 5.5 %collective-permute-start.11 = (bf16[64,768]{1,0:T(8,128)(2,1)S(1)}, bf16[64,768]{1,0:T(8,128)(2,1)S(1)}, u32[]{:S(2)}, u32[]{:S(2)}) collective-permute-start(bf16[64,768]{1,0:T(8,128)(2,1)S(1)} %get-tuple-element.34), channel_id=1, source_target_pairs={{0,2},{2,0},{4,6},{6,4},{8,10},{10,8},{12,14},{14,12},{16,18},{18,... | collective-permute-start | bytes 294920 | tf_op jit(solution)/shard_map/ppermute | solution.py:279
  39.4 3.9 %collective-permute-start.14 = (bf16[32,768]{1,0:T(8,128)(2,1)S(1)}, bf16[32,768]{1,0:T(8,128)(2,1)S(1)}, u32[]{:S(2)}, u32[]{:S(2)}) collective-permute-start(bf16[32,768]{1,0:T(8,128)(2,1)S(1)} %slice.56), channel_id=1, source_target_pairs={{0,9},{1,8},{2,11},{3,10},{4,13},{5,12},{6,15},{7,14},{8,1},{9,0},... | collective-permute-start | bytes 147464 | tf_op jit(solution)/shard_map/ppermute | solution.py:274
  43.4 4.4 %collective-permute-start.15 = (bf16[16,768]{1,0:T(8,128)(2,1)S(1)}, bf16[16,768]{1,0:T(8,128)(2,1)S(1)}, u32[]{:S(2)}, u32[]{:S(2)}) collective-permute-start(bf16[16,768]{1,0:T(8,128)(2,1)S(1)} %slice.57), channel_id=1, source_target_pairs={{0,17},{1,16},{2,19},{3,18},{4,21},{5,20},{6,23},{7,22},{8,25},{9,... | collective-permute-start | bytes 73736 | tf_op jit(solution)/shard_map/ppermute | solution.py:274
where the time goes:
time: 48.5 us; the launch traced here: 48.4 us
  waiting for transfers between devices  19.5 us (40%)
  starting transfers between devices  16 us (33%)
  Pallas kernels  11.2 us (23%)
  between operations  0.82 us (2%)
  other arithmetic  0.77 us (2%)
    ppermute x8, starting transfers between devices, swap_ep(): return lax.ppermute(x, 'ep', [(i, i ^ mask) for i in range(count)])  13.2 us
    ppermute x8, waiting for transfers between devices, swap_ep(): return lax.ppermute(x, 'ep', [(i, i ^ mask) for i in range(count)])  9.46 us
    ppermute x2, waiting for transfers between devices, cross(): return lax.ppermute(x, ('ep', 'tp'), pairs)  6.26 us
    pallas_call x1, Pallas kernels, mixer(): pl.pallas_call(lambda *refs: mixer_body(heads, head_size, *refs), out_sha...  5.41 us
    pallas_call x1, Pallas kernels, update_state(): pl.pallas_call(state_body, grid=(heads,), out_shape=jax.ShapeDtypeStruct(...  4.06 us
    ppermute x6, waiting for transfers between devices, swap_tp(): return lax.ppermute(x, 'tp', [(i, i ^ 1) for i in range(count)])  3.77 us
    ppermute x2, starting transfers between devices, cross(): return lax.ppermute(x, ('ep', 'tp'), pairs)  2.04 us
    pallas_call x1, Pallas kernels, ffn(): pl.pallas_call(lambda *refs: ffn_body(len(near), seqs, top, half, *refs),...  1.53 us
  transfers between devices with their start and end apart: 16, of which 13 were waited for; matrix products, arithmetic and copies ran while one was open for 0% of the time, Pallas kernels for 8%

commit v1 on v0

--- a/solution.py
+++ b/solution.py
@@ -217,9 +217,35 @@
     )(base, other, gain, blend_vector, extra)
 
 
+def prefetch_body(*refs):
+    sources, places, sems = refs[:6], refs[6:9], refs[9]
+    copies = []
+    for at in range(6):
+        count = sources[at].shape[0]
+        copies.append(
+            pltpu.make_async_copy(sources[at], places[at // 2].at[pl.ds(at % 2 * count, count)], sems.at[at])
+        )
+    for copy in copies:
+        copy.start()
+    for copy in copies:
+        copy.wait()
+
+
+def prefetch(weights):
+    return pl.pallas_call(
+        prefetch_body,
+        out_shape=tuple(pltpu.VMEM((2 * w.shape[0], w.shape[1]), w.dtype) for w in weights[::2]),
+        in_specs=[HBM] * 6,
+        out_specs=(VMEM,) * 3,
+        scratch_shapes=[pltpu.SemaphoreType.DMA((6,))],
+        compiler_params=pltpu.CompilerParams(vmem_limit_bytes=4 * MIB),
+        name="prefetch",
+    )(*(in_hbm(w) for w in weights))
+
+
 def ffn_body(pieces, seqs, top, half, *refs):
-    places, blocks = refs[:6], refs[6 : 6 + 2 * pieces]
-    other_ref, mine_ref = refs[6 + 2 * pieces :]
+    places, blocks = refs[:3], refs[3 : 3 + 2 * pieces]
+    other_ref, mine_ref = refs[3 + 2 * pieces :]
     near = jnp.concatenate([b[:, :half] for b in blocks[:pieces]], axis=0)
     far = jnp.concatenate([b[:, :half] for b in blocks[pieces:]], axis=0)
     first = lax.axis_index("tp") == 0
@@ -230,20 +256,18 @@
     scale = jnp.sum(jnp.where(info[:, :top] == here, scalars, 0.0), axis=1, keepdims=True)
     blend = info[:, 3 * top : 3 * top + 1] + info[:, 3 * top + 1 : 3 * top + 2]
 
-    def hidden(at, by):
-        gate = dot_nt(rows, places[at][...])
-        up = dot_nt(rows, places[at + 1][...])
-        return (gate / (1.0 + jnp.exp(-gate)) * up * by).astype(BF)
-
-    expert = hidden(0, scale)
-    dense = hidden(2, blend)
+    gate = dot_nt(rows, places[0][...])
+    up = dot_nt(rows, places[1][...])
+    unit = lax.broadcasted_iota(jnp.int32, gate.shape, 1)
+    by = jnp.where(unit < gate.shape[1] // 2, scale, blend)
+    hidden = (gate / (1.0 + jnp.exp(-gate)) * up * by).astype(BF)
     count = blocks[0].shape[0] // seqs
     chunk = lax.broadcasted_iota(jnp.int32, (near.shape[0], 1), 0) // seqs % count
     side = chunk * 0 + lax.axis_index("tp")
     for bit in range(count.bit_length() - 1):
         side = side ^ (chunk >> bit & 1)
-    low = dot(expert, places[4][:, :half]) + dot(dense, places[5][:, :half])
-    high = dot(expert, places[4][:, half:]) + dot(dense, places[5][:, half:])
+    low = dot(hidden, places[2][:, :half])
+    high = dot(hidden, places[2][:, half:])
     other_ref[...] = jnp.where(side == 0, high, low).astype(BF)
     mine_ref[...] = jnp.where(side == 0, low, high)
 
@@ -330,10 +354,23 @@
     )
     block, resid = pack(base, swap_tp(partial_value), mid_gain, blend_vector, extra, top_count)
 
+    weights = (
+        expert_gate[0].T,
+        dense_gate.T,
+        expert_up[0].T,
+        dense_up.T,
+        expert_down[0],
+        dense_down,
+    )
+    block, *weights = lax.optimization_barrier((block, *weights))
+    weights = prefetch(weights)
     mask = count_ep // 2
     masks = []
     while mask >= 4:
-        block = jnp.concatenate([block, swap_ep(block, mask)], axis=0)
+        arrived = swap_ep(block, mask)
+        if not masks:
+            arrived, *weights = lax.optimization_barrier((arrived, *weights))
+        block = jnp.concatenate([block, arrived], axis=0)
         masks.append(mask)
         mask //= 2
     low = [m for m in (1, 3, 2) if m < count_ep]
@@ -343,14 +380,6 @@
     far = [swap_tp(b) for b in near]
     rows = sum(b.shape[0] for b in near)
 
-    weights = (
-        expert_gate[0].T,
-        expert_up[0].T,
-        dense_gate.T,
-        dense_up.T,
-        expert_down[0],
-        dense_down,
-    )
     other, mine = ffn(weights, near, far, seqs, top_count)
     total = mine + swap_tp(other).astype(F32)
 

time: 48.5 us -> 48.2 us (level)
  waiting for transfers between devices: 19.5 us -> 17.2 us
  Pallas kernels: 11.2 us -> 13.1 us
    pallas_call x0 -> x1, Pallas kernels: none -> 2 us  [prefetch(): pl.pallas_call(prefetch_body, out_shape=tuple((pltpu.VMEM((2 * w.shape[0]...]
    ppermute x8, waiting for transfers between devices: 9.46 us -> 7.61 us  [swap_ep(): return lax.ppermute(x, 'ep', [(i, i ^ mask) for i in range(count)])]
  transfers between devices with their start and end apart: 16 -> 16, of which waited for: 13 -> 12; matrix products, arithmetic and copies ran while one was open for 0% -> 0% of each run, Pallas kernels for 8% -> 13%
where the time goes in v1:
time: 48.2 us; the launch traced here: 48 us
  waiting for transfers between devices  17.2 us (36%)
  starting transfers between devices  16.1 us (33%)
  Pallas kernels  13.1 us (27%)
  other arithmetic  0.77 us (2%)
  between operations  0.75 us (2%)
    ppermute x8, starting transfers between devices, swap_ep(): return lax.ppermute(x, 'ep', [(i, i ^ mask) for i in range(count)])  12.8 us
    ppermute x8, waiting for transfers between devices, swap_ep(): return lax.ppermute(x, 'ep', [(i, i ^ mask) for i in range(count)])  7.61 us
    ppermute x2, waiting for transfers between devices, cross(): return lax.ppermute(x, ('ep', 'tp'), pairs)  6.19 us
    pallas_call x1, Pallas kernels, mixer(): pl.pallas_call(lambda *refs: mixer_body(heads, head_size, *refs), out_sha...  5.29 us
    pallas_call x1, Pallas kernels, update_state(): pl.pallas_call(state_body, grid=(heads,), out_shape=jax.ShapeDtypeStruct(...  4.06 us
    ppermute x6, waiting for transfers between devices, swap_tp(): return lax.ppermute(x, 'tp', [(i, i ^ 1) for i in range(count)])  3.37 us
    ppermute x2, starting transfers between devices, cross(): return lax.ppermute(x, ('ep', 'tp'), pairs)  2.13 us
    pallas_call x1, Pallas kernels, prefetch(): pl.pallas_call(prefetch_body, out_shape=tuple((pltpu.VMEM((2 * w.shape[0]...  2 us
  transfers between devices with their start and end apart: 16, of which 12 were waited for; matrix products, arithmetic and copies ran while one was open for 0% of the time, Pallas kernels for 13%

profile of v1, /device:TPU:0, one launch (start us, length us, event | category | flops | bytes accessed | tf_op | source)
XLA Modules:
  0.0 48.0 jit_solution(9072225907711500651)
XLA Ops:
  0.7 5.3 %mixer.1 = (bf16[16,1536]{1,0:T(8,128)(2,1)S(1)}, f32[16,1536]{1,0:T(8,128)S(1)}, f32[5,6,16,64]{3,2,1,0:T(8,128)S(1)}, bf16[16,128]{1,0:T(8,128)(2,1)S(1)}) custom-call(bf16[16,1536]{1,0:T(8,128)(2,1)} %refs_0_.1, f32[1536]{0:T(1024)} %refs_1_.1, s32[6,16]{1,0:T(8,128)} %bitcast.28, f32[6,16]{1,0:T(8,128)} %bitcast.29, bf16[1536,384]{1,0:T(8,128)(2,1)} %refs_4_.1, ...), custom_call_target="tpu_custom_call" | custom-call | tf_op jit(solution)/shard_map/mixer/pallas_call | solution.py:142
  6.0 0.6 %collective-permute-start = (bf16[16,1536]{1,0:T(8,128)(2,1)S(1)}, bf16[16,1536]{1,0:T(8,128)(2,1)S(1)}, u32[]{:S(2)}, u32[]{:S(2)}) collective-permute-start(bf16[16,1536]{1,0:T(8,128)(2,1)S(1)} %get-tuple-element.31), channel_id=1, source_target_pairs={{0,1},{1,0},{2,3},{3,2},{4,5},{5,4},{6,7},{7,6},{8,9},{9,8},{10,11... | collective-permute-start | bytes 147464 | tf_op jit(solution)/shard_map/ppermute | solution.py:290
  6.5 0.9 %collective-permute-done.refs_1_ = bf16[16,1536]{1,0:T(8,128)(2,1)S(1)} collective-permute-done((bf16[16,1536]{1,0:T(8,128)(2,1)S(1)}, bf16[16,1536]{1,0:T(8,128)(2,1)S(1)}, u32[]{:S(2)}, u32[]{:S(2)}) %collective-permute-start) | collective-permute-done | bytes 49184 | tf_op jit(solution)/shard_map/ppermute | solution.py:290
  7.4 0.2 pack.1
  7.6 4.0 %collective-permute-start.1 = (bf16[16,896]{1,0:T(8,128)(2,1)S(1)}, bf16[16,896]{1,0:T(8,128)(2,1)S(1)}, u32[]{:S(2)}, u32[]{:S(2)}) collective-permute-start(bf16[16,896]{1,0:T(8,128)(2,1)S(1)} %get-tuple-element.35), channel_id=1, source_target_pairs={{0,16},{2,18},{4,20},{6,22},{8,24},{10,26},{12,28},{14,30},{16,0},... | collective-permute-start | bytes 86024 | tf_op jit(solution)/shard_map/ppermute | solution.py:303
  11.6 2.0 %prefetch.1 = (bf16[384,1536]{1,0:T(8,128)(2,1)S(1)}, bf16[384,1536]{1,0:T(8,128)(2,1)S(1)}, bf16[384,1536]{1,0:T(8,128)(2,1)S(1)}) custom-call(bf16[192,1536]{1,0:T(8,128)(2,1)} %bitcast.21, bf16[192,1536]{1,0:T(8,128)(2,1)} %bitcast.22, bf16[192,1536]{1,0:T(8,128)(2,1)} %bitcast.23, bf16[192,1536]{1,0:T(8,128)(2,1)} %bitcast.24, ...), custom_call_target="tpu_custom_call" | custom-call | tf_op jit(solution)/shard_map/prefetch/pallas_call | solution.py:235
  13.6 1.7 %collective-permute-start.2 = (bf16[32,896]{1,0:T(8,128)(2,1)S(1)}, bf16[32,896]{1,0:T(8,128)(2,1)S(1)}, u32[]{:S(2)}, u32[]{:S(2)}) collective-permute-start(bf16[32,896]{1,0:T(8,128)(2,1)S(1)} %pad_maximum_fusion), channel_id=1, source_target_pairs={{0,8},{2,10},{4,12},{6,14},{8,0},{10,2},{12,4},{14,6},{16,24},{18,... | collective-permute-start | bytes 172040 | tf_op jit(solution)/shard_map/ppermute | solution.py:303
  15.4 2.5 %collective-permute-done.2 = bf16[32,896]{1,0:T(8,128)(2,1)S(1)} collective-permute-done((bf16[32,896]{1,0:T(8,128)(2,1)S(1)}, bf16[32,896]{1,0:T(8,128)(2,1)S(1)}, u32[]{:S(2)}, u32[]{:S(2)}) %collective-permute-start.2) | collective-permute-done | bytes 57376 | tf_op jit(solution)/shard_map/ppermute | solution.py:303
  17.9 2.0 %collective-permute-start.5 = (bf16[64,896]{1,0:T(8,128)(2,1)S(1)}, bf16[64,896]{1,0:T(8,128)(2,1)S(1)}, u32[]{:S(2)}, u32[]{:S(2)}) collective-permute-start(bf16[64,896]{1,0:T(8,128)(2,1)S(1)} %constant_dynamic-update-slice_fusion.refs_3_), channel_id=1, source_target_pairs={{0,4},{2,6},{4,0},{6,2},{8,12},{10,14},{12,8},{14,10},{16,20},{18,... | collective-permute-start | bytes 344072 | tf_op jit(solution)/shard_map/ppermute | solution.py:303
  19.9 1.1 %collective-permute-start.4 = (bf16[64,896]{1,0:T(8,128)(2,1)S(1)}, bf16[64,896]{1,0:T(8,128)(2,1)S(1)}, u32[]{:S(2)}, u32[]{:S(2)}) collective-permute-start(bf16[64,896]{1,0:T(8,128)(2,1)S(1)} %constant_dynamic-update-slice_fusion.refs_3_), channel_id=1, source_target_pairs={{0,6},{2,4},{4,2},{6,0},{8,14},{10,12},{12,10},{14,8},{16,22},{18,... | collective-permute-start | bytes 344072 | tf_op jit(solution)/shard_map/ppermute | solution.py:303
  21.0 0.5 collective-permute-start.3
  21.5 2.4 %collective-permute-done.5.refs_6_ = bf16[64,896]{1,0:T(8,128)(2,1)S(1)} collective-permute-done((bf16[64,896]{1,0:T(8,128)(2,1)S(1)}, bf16[64,896]{1,0:T(8,128)(2,1)S(1)}, u32[]{:S(2)}, u32[]{:S(2)}) %collective-permute-start.5) | collective-permute-done | bytes 114720 | tf_op jit(solution)/shard_map/ppermute | solution.py:303
  23.9 1.7 %collective-permute-done.4.refs_5_ = bf16[64,896]{1,0:T(8,128)(2,1)S(1)} collective-permute-done((bf16[64,896]{1,0:T(8,128)(2,1)S(1)}, bf16[64,896]{1,0:T(8,128)(2,1)S(1)}, u32[]{:S(2)}, u32[]{:S(2)}) %collective-permute-start.4) | collective-permute-done | bytes 114720 | tf_op jit(solution)/shard_map/ppermute | solution.py:303
  25.6 0.2 collective-permute-done.3.refs_4_
  25.8 0.3 collective-permute-start.7
  26.1 0.8 %collective-permute-done.8.refs_9_ = bf16[64,896]{1,0:T(8,128)(2,1)S(1)} collective-permute-done((bf16[64,896]{1,0:T(8,128)(2,1)S(1)}, bf16[64,896]{1,0:T(8,128)(2,1)S(1)}, u32[]{:S(2)}, u32[]{:S(2)}) %collective-permute-start.8) | collective-permute-done | bytes 114720 | tf_op jit(solution)/shard_map/ppermute | solution.py:290
  26.9 0.2 collective-permute-done.7.refs_8_
  27.1 1.5 %ffn.1 = (bf16[256,768]{1,0:T(8,128)(2,1)S(1)}, f32[256,768]{1,0:T(8,128)S(1)}) custom-call(bf16[384,1536]{1,0:T(8,128)(2,1)S(1)} %get-tuple-element.45.refs_0_, bf16[384,1536]{1,0:T(8,128)(2,1)S(1)} %get-tuple-element.46.refs_1_, bf16[384,1536]{1,0:T(8,128)(2,1)S(1)} %get-tuple-element.47.refs_2_, ...), custom_call_target="tpu_custom_call" | custom-call | tf_op jit(solution)/shard_map/ffn/pallas_call | solution.py:278
  28.6 0.3 collective-permute-start.10
  29.0 1.4 %collective-permute-done.10 = bf16[256,768]{1,0:T(8,128)(2,1)S(1)} collective-permute-done((bf16[256,768]{1,0:T(8,128)(2,1)S(1)}, bf16[256,768]{1,0:T(8,128)(2,1)S(1)}, u32[]{:S(2)}, u32[]{:S(2)}) %collective-permute-start.10) | collective-permute-done | bytes 393248 | tf_op jit(solution)/shard_map/ppermute | solution.py:290
  30.4 0.1 fusion.2
  30.5 1.6 %collective-permute-start.13 = (bf16[64,768]{1,0:T(8,128)(2,1)S(1)}, bf16[64,768]{1,0:T(8,128)(2,1)S(1)}, u32[]{:S(2)}, u32[]{:S(2)}) collective-permute-start(bf16[64,768]{1,0:T(8,128)(2,1)S(1)} %get-tuple-element.60), channel_id=1, source_target_pairs={{0,4},{2,6},{4,0},{6,2},{8,12},{10,14},{12,8},{14,10},{16,20},{18,... | collective-permute-start | bytes 294920 | tf_op jit(solution)/shard_map/ppermute | solution.py:303
  32.2 1.1 %collective-permute-start.12 = (bf16[64,768]{1,0:T(8,128)(2,1)S(1)}, bf16[64,768]{1,0:T(8,128)(2,1)S(1)}, u32[]{:S(2)}, u32[]{:S(2)}) collective-permute-start(bf16[64,768]{1,0:T(8,128)(2,1)S(1)} %get-tuple-element.61), channel_id=1, source_target_pairs={{0,6},{2,4},{4,2},{6,0},{8,14},{10,12},{12,10},{14,8},{16,22},{18,... | collective-permute-start | bytes 294920 | tf_op jit(solution)/shard_map/ppermute | solution.py:303
  33.3 0.8 %collective-permute-start.11 = (bf16[64,768]{1,0:T(8,128)(2,1)S(1)}, bf16[64,768]{1,0:T(8,128)(2,1)S(1)}, u32[]{:S(2)}, u32[]{:S(2)}) collective-permute-start(bf16[64,768]{1,0:T(8,128)(2,1)S(1)} %get-tuple-element.62), channel_id=1, source_target_pairs={{0,2},{2,0},{4,6},{6,4},{8,10},{10,8},{12,14},{14,12},{16,18},{18,... | collective-permute-start | bytes 294920 | tf_op jit(solution)/shard_map/ppermute | solution.py:303
  34.1 4.1 %state_update.1 = f32[16,6,64,64]{3,2,1,0:T(8,128)} custom-call(f32[16,6,64,64]{3,2,1,0:T(8,128)S(1)} %copy-done, f32[5,6,16,64]{3,2,1,0:T(8,128)S(1)} %get-tuple-element.53.aux_ref), custom_call_target="tpu_custom_call" | custom-call | flops 100663296 | bytes 6291456 | tf_op jit(solution)/shard_map/state_update/pallas_call | solution.py:176
  38.2 0.5 %collective-permute-done.12 = bf16[64,768]{1,0:T(8,128)(2,1)S(1)} collective-permute-done((bf16[64,768]{1,0:T(8,128)(2,1)S(1)}, bf16[64,768]{1,0:T(8,128)(2,1)S(1)}, u32[]{:S(2)}, u32[]{:S(2)}) %collective-permute-start.12) | collective-permute-done | bytes 98336 | tf_op jit(solution)/shard_map/ppermute | solution.py:303
  38.7 0.2 collective-permute-done.11
  39.0 0.2 collective-permute-start.14
  39.2 3.9 %collective-permute-done.14 = bf16[32,768]{1,0:T(8,128)(2,1)S(1)} collective-permute-done((bf16[32,768]{1,0:T(8,128)(2,1)S(1)}, bf16[32,768]{1,0:T(8,128)(2,1)S(1)}, u32[]{:S(2)}, u32[]{:S(2)}) %collective-permute-start.14) | collective-permute-done | bytes 49184 | tf_op jit(solution)/shard_map/ppermute | solution.py:298
  43.1 2.0 %collective-permute-start.15 = (bf16[16,768]{1,0:T(8,128)(2,1)S(1)}, bf16[16,768]{1,0:T(8,128)(2,1)S(1)}, u32[]{:S(2)}, u32[]{:S(2)}) collective-permute-start(bf16[16,768]{1,0:T(8,128)(2,1)S(1)} %slice.57), channel_id=1, source_target_pairs={{0,17},{1,16},{2,19},{3,18},{4,21},{5,20},{6,23},{7,22},{8,25},{9,... | collective-permute-start | bytes 73736 | tf_op jit(solution)/shard_map/ppermute | solution.py:298
  45.1 2.3 %collective-permute-done.15 = bf16[16,768]{1,0:T(8,128)(2,1)S(1)} collective-permute-done((bf16[16,768]{1,0:T(8,128)(2,1)S(1)}, bf16[16,768]{1,0:T(8,128)(2,1)S(1)}, u32[]{:S(2)}, u32[]{:S(2)}) %collective-permute-start.15) | collective-permute-done | bytes 24608 | tf_op jit(solution)/shard_map/ppermute | solution.py:298
  47.3 0.6 %fusion.1 = bf16[16,768]{1,0:T(8,128)(2,1)} fusion(f32[16,768]{1,0:T(8,128)S(1)} %get-tuple-element.33, f32[32,768]{1,0:T(8,128)S(1)} %slice_add_fusion.1, bf16[16,768]{1,0:T(8,128)(2,1)S(1)} %collective-permute-done.15), kind=kLoop, calls=%fused_computation.11 | loop fusion | flops 49152 | bytes 147456 | tf_op jit(solution)/shard_map/convert_element_type | solution.py:399
  (22 shorter events, 0.1 us)
Async XLA Ops:
  0.6 6.8 %copy-start.1 = (f32[1536]{0:T(1024)S(1)}, f32[1536]{0:T(1024)}, u32[]{:S(2)}) copy-start(f32[1536]{0:T(1024)} %refs_2_.1) | copy-start | bytes 18436
  0.6 6.8 %copy-start.2 = (bf16[1536]{0:T(1024)(128)(2,1)S(1)}, bf16[1536]{0:T(1024)(128)(2,1)}, u32[]{:S(2)}) copy-start(bf16[1536]{0:T(1024)(128)(2,1)} %refs_3_.1) | copy-start | bytes 9220
  6.0 1.4 %collective-permute-start = (bf16[16,1536]{1,0:T(8,128)(2,1)S(1)}, bf16[16,1536]{1,0:T(8,128)(2,1)S(1)}, u32[]{:S(2)}, u32[]{:S(2)}) collective-permute-start(bf16[16,1536]{1,0:T(8,128)(2,1)S(1)} %get-tuple-element.31), channel_id=1, source_target_pairs={{0,1},{1,0},{2,3},{3,2},{4,5},{5,4},{6,7},{7,6},{8,9},{9,8},{10,11... | collective-permute-start | bytes 147464 | tf_op jit(solution)/shard_map/ppermute | solution.py:290
  7.6 6.0 %collective-permute-start.1 = (bf16[16,896]{1,0:T(8,128)(2,1)S(1)}, bf16[16,896]{1,0:T(8,128)(2,1)S(1)}, u32[]{:S(2)}, u32[]{:S(2)}) collective-permute-start(bf16[16,896]{1,0:T(8,128)(2,1)S(1)} %get-tuple-element.35), channel_id=1, source_target_pairs={{0,16},{2,18},{4,20},{6,22},{8,24},{10,26},{12,28},{14,30},{16,0},... | collective-permute-start | bytes 86024 | tf_op jit(solution)/shard_map/ppermute | solution.py:303
  13.6 4.2 %collective-permute-start.2 = (bf16[32,896]{1,0:T(8,128)(2,1)S(1)}, bf16[32,896]{1,0:T(8,128)(2,1)S(1)}, u32[]{:S(2)}, u32[]{:S(2)}) collective-permute-start(bf16[32,896]{1,0:T(8,128)(2,1)S(1)} %pad_maximum_fusion), channel_id=1, source_target_pairs={{0,8},{2,10},{4,12},{6,14},{8,0},{10,2},{12,4},{14,6},{16,24},{18,... | collective-permute-start | bytes 172040 | tf_op jit(solution)/shard_map/ppermute | solution.py:303
  17.9 6.0 %collective-permute-start.5 = (bf16[64,896]{1,0:T(8,128)(2,1)S(1)}, bf16[64,896]{1,0:T(8,128)(2,1)S(1)}, u32[]{:S(2)}, u32[]{:S(2)}) collective-permute-start(bf16[64,896]{1,0:T(8,128)(2,1)S(1)} %constant_dynamic-update-slice_fusion.refs_3_), channel_id=1, source_target_pairs={{0,4},{2,6},{4,0},{6,2},{8,12},{10,14},{12,8},{14,10},{16,20},{18,... | collective-permute-start | bytes 344072 | tf_op jit(solution)/shard_map/ppermute | solution.py:303
  19.9 5.7 %collective-permute-start.4 = (bf16[64,896]{1,0:T(8,128)(2,1)S(1)}, bf16[64,896]{1,0:T(8,128)(2,1)S(1)}, u32[]{:S(2)}, u32[]{:S(2)}) collective-permute-start(bf16[64,896]{1,0:T(8,128)(2,1)S(1)} %constant_dynamic-update-slice_fusion.refs_3_), channel_id=1, source_target_pairs={{0,6},{2,4},{4,2},{6,0},{8,14},{10,12},{12,10},{14,8},{16,22},{18,... | collective-permute-start | bytes 344072 | tf_op jit(solution)/shard_map/ppermute | solution.py:303
  21.0 4.8 %collective-permute-start.3 = (bf16[64,896]{1,0:T(8,128)(2,1)S(1)}, bf16[64,896]{1,0:T(8,128)(2,1)S(1)}, u32[]{:S(2)}, u32[]{:S(2)}) collective-permute-start(bf16[64,896]{1,0:T(8,128)(2,1)S(1)} %constant_dynamic-update-slice_fusion.refs_3_), channel_id=1, source_target_pairs={{0,2},{2,0},{4,6},{6,4},{8,10},{10,8},{12,14},{14,12},{16,18},{18,... | collective-permute-start | bytes 344072 | tf_op jit(solution)/shard_map/ppermute | solution.py:303
  21.5 4.6 %collective-permute-start.6 = (bf16[64,896]{1,0:T(8,128)(2,1)S(1)}, bf16[64,896]{1,0:T(8,128)(2,1)S(1)}, u32[]{:S(2)}, u32[]{:S(2)}) collective-permute-start(bf16[64,896]{1,0:T(8,128)(2,1)S(1)} %constant_dynamic-update-slice_fusion.refs_3_), channel_id=1, source_target_pairs={{0,1},{1,0},{2,3},{3,2},{4,5},{5,4},{6,7},{7,6},{8,9},{9,8},{10,11... | collective-permute-start | bytes 344072 | tf_op jit(solution)/shard_map/ppermute | solution.py:290
  23.9 2.2 %collective-permute-start.9 = (bf16[64,896]{1,0:T(8,128)(2,1)S(1)}, bf16[64,896]{1,0:T(8,128)(2,1)S(1)}, u32[]{:S(2)}, u32[]{:S(2)}) collective-permute-start(bf16[64,896]{1,0:T(8,128)(2,1)S(1)} %collective-permute-done.5.refs_6_), channel_id=1, source_target_pairs={{0,1},{1,0},{2,3},{3,2},{4,5},{5,4},{6,7},{7,6},{8,9},{9,8},{10,11... | collective-permute-start | bytes 344072 | tf_op jit(solution)/shard_map/ppermute | solution.py:290
  25.6 1.3 %collective-permute-start.8 = (bf16[64,896]{1,0:T(8,128)(2,1)S(1)}, bf16[64,896]{1,0:T(8,128)(2,1)S(1)}, u32[]{:S(2)}, u32[]{:S(2)}) collective-permute-start(bf16[64,896]{1,0:T(8,128)(2,1)S(1)} %collective-permute-done.4.refs_5_), channel_id=1, source_target_pairs={{0,1},{1,0},{2,3},{3,2},{4,5},{5,4},{6,7},{7,6},{8,9},{9,8},{10,11... | collective-permute-start | bytes 344072 | tf_op jit(solution)/shard_map/ppermute | solution.py:290
  25.8 1.3 %collective-permute-start.7 = (bf16[64,896]{1,0:T(8,128)(2,1)S(1)}, bf16[64,896]{1,0:T(8,128)(2,1)S(1)}, u32[]{:S(2)}, u32[]{:S(2)}) collective-permute-start(bf16[64,896]{1,0:T(8,128)(2,1)S(1)} %collective-permute-done.3.refs_4_), channel_id=1, source_target_pairs={{0,1},{1,0},{2,3},{3,2},{4,5},{5,4},{6,7},{7,6},{8,9},{9,8},{10,11... | collective-permute-start | bytes 344072 | tf_op jit(solution)/shard_map/ppermute | solution.py:290
  27.1 7.0 %copy-start = (f32[16,6,64,64]{3,2,1,0:T(8,128)S(1)}, f32[16,6,64,64]{3,2,1,0:T(8,128)}, u32[]{:S(2)}) copy-start(f32[16,6,64,64]{3,2,1,0:T(8,128)} %state_ref.1) | copy-start | bytes 4718596
  28.6 1.8 %collective-permute-start.10 = (bf16[256,768]{1,0:T(8,128)(2,1)S(1)}, bf16[256,768]{1,0:T(8,128)(2,1)S(1)}, u32[]{:S(2)}, u32[]{:S(2)}) collective-permute-start(bf16[256,768]{1,0:T(8,128)(2,1)S(1)} %get-tuple-element.50), channel_id=1, source_target_pairs={{0,1},{1,0},{2,3},{3,2},{4,5},{5,4},{6,7},{7,6},{8,9},{9,8},{10,11... | collective-permute-start | bytes 1179656 | tf_op jit(solution)/shard_map/ppermute | solution.py:290
  30.5 7.6 %collective-permute-start.13 = (bf16[64,768]{1,0:T(8,128)(2,1)S(1)}, bf16[64,768]{1,0:T(8,128)(2,1)S(1)}, u32[]{:S(2)}, u32[]{:S(2)}) collective-permute-start(bf16[64,768]{1,0:T(8,128)(2,1)S(1)} %get-tuple-element.60), channel_id=1, source_target_pairs={{0,4},{2,6},{4,0},{6,2},{8,12},{10,14},{12,8},{14,10},{16,20},{18,... | collective-permute-start | bytes 294920 | tf_op jit(solution)/shard_map/ppermute | solution.py:303
  32.2 6.5 %collective-permute-start.12 = (bf16[64,768]{1,0:T(8,128)(2,1)S(1)}, bf16[64,768]{1,0:T(8,128)(2,1)S(1)}, u32[]{:S(2)}, u32[]{:S(2)}) collective-permute-start(bf16[64,768]{1,0:T(8,128)(2,1)S(1)} %get-tuple-element.61), channel_id=1, source_target_pairs={{0,6},{2,4},{4,2},{6,0},{8,14},{10,12},{12,10},{14,8},{16,22},{18,... | collective-permute-start | bytes 294920 | tf_op jit(solution)/shard_map/ppermute | solution.py:303
  33.3 5.6 %collective-permute-start.11 = (bf16[64,768]{1,0:T(8,128)(2,1)S(1)}, bf16[64,768]{1,0:T(8,128)(2,1)S(1)}, u32[]{:S(2)}, u32[]{:S(2)}) collective-permute-start(bf16[64,768]{1,0:T(8,128)(2,1)S(1)} %get-tuple-element.62), channel_id=1, source_target_pairs={{0,2},{2,0},{4,6},{6,4},{8,10},{10,8},{12,14},{14,12},{16,18},{18,... | collective-permute-start | bytes 294920 | tf_op jit(solution)/shard_map/ppermute | solution.py:303
  39.0 4.1 %collective-permute-start.14 = (bf16[32,768]{1,0:T(8,128)(2,1)S(1)}, bf16[32,768]{1,0:T(8,128)(2,1)S(1)}, u32[]{:S(2)}, u32[]{:S(2)}) collective-permute-start(bf16[32,768]{1,0:T(8,128)(2,1)S(1)} %slice.56), channel_id=1, source_target_pairs={{0,9},{1,8},{2,11},{3,10},{4,13},{5,12},{6,15},{7,14},{8,1},{9,0},... | collective-permute-start | bytes 147464 | tf_op jit(solution)/shard_map/ppermute | solution.py:298
  43.1 4.2 %collective-permute-start.15 = (bf16[16,768]{1,0:T(8,128)(2,1)S(1)}, bf16[16,768]{1,0:T(8,128)(2,1)S(1)}, u32[]{:S(2)}, u32[]{:S(2)}) collective-permute-start(bf16[16,768]{1,0:T(8,128)(2,1)S(1)} %slice.57), channel_id=1, source_target_pairs={{0,17},{1,16},{2,19},{3,18},{4,21},{5,20},{6,23},{7,22},{8,25},{9,... | collective-permute-start | bytes 73736 | tf_op jit(solution)/shard_map/ppermute | solution.py:298
